TPU v7x, 256 devices: a whole 4x4x8 slice. The times are simulated.
256 devices in a mesh: kv: 16 (over y, x), tp: 16 (over z, core).
Axes of the slice: x: 4, y: 4, z: 8, core: 2. Of those that a mesh axis runs over, the one named last changes fastest.
Arguments:
- tokens: bfloat16 [128, 4096], P(None, ('kv', 'tp')), may hold values from -41 to 41
- lengths: int32 [128], P('kv'), may hold values from 1 to 8192, 262144 in all
- retention_state: float32 [128, 16, 128, 256], P('kv', 'tp'), may hold values from -4 to 4
- mixer_gain: float32 [4096], P('kv'), may hold values from 0.1 to 1.9
- query_weight: bfloat16 [4096, 2048], P('kv', 'tp'), may hold values from -0.09375 to 0.09375
- key_weight: bfloat16 [4096, 2048], P('kv', 'tp'), may hold values from -0.09375 to 0.09375
- value_weight: bfloat16 [4096, 4096], P('kv', 'tp'), may hold values from -0.09375 to 0.09375
- gate_weight: bfloat16 [4096, 4096], P('kv', 'tp'), may hold values from -0.09375 to 0.09375
- output_weight: bfloat16 [4096, 4096], P('tp', 'kv'), may hold values from -0.125 to 0.125
- channel_gain: float32 [4096], P('kv'), may hold values from 0.1 to 1.9
- ffn_gate: bfloat16 [4096, 11264], P('kv', 'tp'), may hold values from -0.09375 to 0.09375
- ffn_up: bfloat16 [4096, 11264], P('kv', 'tp'), may hold values from -0.09375 to 0.09375
- ffn_down: bfloat16 [11264, 4096], P('tp', 'kv'), may hold values from -0.078125 to 0.078125
Outputs:
- layer_output: bfloat16 [128, 4096], P(None, ('kv', 'tp'))
- new_state: float32 [128, 16, 128, 256], P('kv', 'tp')
All inputs are finite; a program needn't handle non-finite values. No bound on the sum of `lengths` on one device may be relied on, other than what follows from the above.
Results may differ from a plain program's by a relative error of at most 0.022.
Values may be sent and summed in bfloat16 or wider, within the bound.
No kernel may reach another device: no remote copies, remote signals or barrier semaphores. Data moves between devices by JAX's collectives and lax.ppermute only.
A program may use at most 64 MiB of HBM per device.

v0:
```python
import jax
import jax.numpy as jnp
from jax import lax
from jax.sharding import PartitionSpec as P

D = 4096
HEADS = 16
QK = 128


def in_blocks(value, dim, devices):
    lengths = value.shape
    blocks = value.reshape(*lengths[:dim], devices, lengths[dim] // devices, *lengths[dim + 1 :])
    return jnp.moveaxis(blocks, dim, 0)


def sent_and_summed(value, axis, dim):
    blocks = in_blocks(value, dim, lax.axis_size(axis))
    arrived = lax.all_to_all(blocks, axis, split_axis=0, concat_axis=0, tiled=True)
    return arrived.astype(jnp.float32).sum(axis=0)


def in_one_piece(arrays, axis, dim, along):
    columns = [a.reshape(*a.shape[:along], -1) for a in arrays]
    both = jnp.concatenate(columns, axis=along)
    result, at, finished = (sent_and_summed(both, axis, dim), 0, [])
    for a, column in zip(arrays, columns):
        piece = result[..., at : at + column.shape[along]]
        finished.append(piece.reshape(*piece.shape[:along], *a.shape[along:]))
        at += column.shape[along]
    return tuple(finished)


def copy_for_each(value, axis):
    devices = lax.axis_size(axis)
    return lax.all_to_all(
        jnp.broadcast_to(value[None], (devices, *value.shape)), axis, 0, 0, tiled=True
    )


def joined_along(blocks, dim):
    blocks = jnp.moveaxis(blocks, 0, dim)
    lengths = blocks.shape
    return blocks.reshape(*lengths[:dim], lengths[dim] * lengths[dim + 1], *lengths[dim + 2 :])


def gather_directly(value, axis, dim):
    blocks = copy_for_each(value, axis)
    return joined_along(blocks, dim)


def rotate_heads(vectors, positions):
    half_dim = vectors.shape[-1] // 2
    frequency = 10000.0 ** (-jnp.arange(half_dim, dtype=jnp.float32) / half_dim)
    angles = positions.astype(jnp.float32)[:, None, None] * frequency
    cosine = jnp.cos(angles)
    sine_part = jnp.sin(angles)
    first_half = vectors[..., :half_dim]
    second = vectors[..., half_dim:]
    return jnp.concatenate(
        [first_half * cosine - second * sine_part, first_half * sine_part + second * cosine],
        axis=-1,
    )


def gathered_rows(columns):
    return lax.all_gather(columns, "tp", axis=1, tiled=True)


def owned_sums(partial_value, squares):
    raw_sums, totals = in_one_piece(
        (partial_value.astype(jnp.bfloat16), squares.astype(jnp.bfloat16)), "kv", 0, 1
    )
    summed = raw_sums * lax.rsqrt(totals / D + 1e-06)[:, None]
    return summed


def on_device(
    tokens,
    lengths,
    retention_state,
    mixer_gain,
    query_weight,
    key_weight,
    value_weight,
    gate_weight,
    output_weight,
    channel_gain,
    ffn_gate,
    ffn_up,
    ffn_down,
):
    feature_block = gathered_rows(tokens).astype(jnp.float32)
    squares = jnp.sum(feature_block * feature_block, axis=1)
    normed = (feature_block * mixer_gain).astype(jnp.bfloat16)
    partial_value = jnp.concatenate(
        [
            jnp.dot(normed, query_weight, preferred_element_type=jnp.float32),
            jnp.dot(normed, key_weight, preferred_element_type=jnp.float32),
            jnp.dot(normed, value_weight, preferred_element_type=jnp.float32),
            jnp.dot(normed, gate_weight, preferred_element_type=jnp.float32),
        ],
        axis=1,
    )
    owned_rows = owned_sums(partial_value, squares)
    local_heads = query_weight.shape[1] // QK
    q_width = query_weight.shape[1]
    v_width = value_weight.shape[1]
    head_width = v_width // local_heads
    seq_rows = owned_rows.shape[0]
    query_rows = rotate_heads(
        owned_rows[:, :q_width].reshape(seq_rows, local_heads, QK), lengths
    ).astype(jnp.bfloat16)
    key_rows = (
        rotate_heads(
            owned_rows[:, q_width : 2 * q_width].reshape(seq_rows, local_heads, QK), lengths
        )
        * QK ** (-0.5)
    ).astype(jnp.bfloat16)
    value_rows = (
        owned_rows[:, 2 * q_width : 2 * q_width + v_width]
        .astype(jnp.bfloat16)
        .reshape(seq_rows, local_heads, head_width)
    )
    gate_rows = owned_rows[:, 2 * q_width + v_width :]
    head_ids = (lax.axis_index("tp") * local_heads + jnp.arange(local_heads)).astype(jnp.float32)
    decay_rate = 1.0 - 2.0 ** (-5.0 - 10.0 * head_ids / (HEADS - 1))
    new_state = (
        decay_rate[None, :, None, None] * retention_state
        + key_rows.astype(jnp.float32)[..., :, None] * value_rows.astype(jnp.float32)[..., None, :]
    )
    retained = jnp.einsum(
        "bhk,bhkv->bhv", query_rows.astype(jnp.float32), new_state, precision=lax.Precision.HIGHEST
    )
    normalized = retained * lax.rsqrt(jnp.mean(retained * retained, axis=-1) + 1e-06)[..., None]
    merged = (normalized.reshape(seq_rows, v_width) * jax.nn.silu(gate_rows)).astype(jnp.bfloat16)
    mixed_part = jnp.dot(
        gather_directly(merged, "kv", 0), output_weight, preferred_element_type=jnp.float32
    )
    mixed_cols = sent_and_summed(mixed_part.astype(jnp.bfloat16), "tp", 1)
    residual = (tokens.astype(jnp.float32) + mixed_cols).astype(jnp.bfloat16)
    block_two = gathered_rows(residual).astype(jnp.float32)
    squares_two = jnp.sum(block_two * block_two, axis=1)
    normed_two = (block_two * channel_gain).astype(jnp.bfloat16)
    partial_two = jnp.concatenate(
        [
            jnp.dot(normed_two, ffn_gate, preferred_element_type=jnp.float32),
            jnp.dot(normed_two, ffn_up, preferred_element_type=jnp.float32),
        ],
        axis=1,
    )
    hidden_units = ffn_gate.shape[1]
    summed = owned_sums(partial_two, squares_two)
    hidden = (jax.nn.silu(summed[:, :hidden_units]) * summed[:, hidden_units:]).astype(jnp.bfloat16)
    down_part = jnp.dot(
        gather_directly(hidden, "kv", 0), ffn_down, preferred_element_type=jnp.float32
    )
    down_sums = sent_and_summed(down_part.astype(jnp.bfloat16), "tp", 1)
    layer_output = (residual.astype(jnp.float32) + down_sums).astype(jnp.bfloat16)
    return (layer_output, new_state)


def solution(mesh):
    in_specs = (
        P(None, ("kv", "tp")),
        P("kv"),
        P("kv", "tp", None, None),
        P("kv"),
        P("kv", "tp"),
        P("kv", "tp"),
        P("kv", "tp"),
        P("kv", "tp"),
        P("tp", "kv"),
        P("kv"),
        P("kv", "tp"),
        P("kv", "tp"),
        P("tp", "kv"),
    )
    out_specs = (P(None, ("kv", "tp")), P("kv", "tp", None, None))
    return jax.shard_map(
        on_device, mesh=mesh, in_specs=in_specs, out_specs=out_specs, check_vma=False
    )
```

profile of v0, /device:TPU:1, one launch (start us, length us, event | category | flops | bytes accessed | tf_op | source)
XLA Modules:
  0.0 126.4 jit_solution(4354620266394448964)
XLA Ops:
  0.6 0.0 copy-start
  0.6 0.0 copy-start.2
  0.7 21.8 %all_gather.6 = bf16[128,256]{0,1:T(8,128)(2,1)S(1)} all-gather(bf16[128,16]{0,1:T(8,128)(2,1)} %param.13), channel_id=1, replica_groups=mesh['kv'=16,'tp'=16] {'tp'}, dimensions={1}, use_global_device_ids=true | all-gather | bytes 69632 | tf_op jit(solution)/shard_map/all_gather | solution.py:67
  22.5 0.1 fusion.12
  22.6 0.2 convert_element_type.141
  22.8 1.8 %fusion.5 = bf16[16,8,769]{2,1,0:T(8,128)(2,1)} fusion(bf16[256,128]{1,0:T(8,128)(2,1)} %param.17, bf16[128,256]{0,1:T(8,128)(2,1)S(1)} %all_gather.6, f32[256]{0:T(256)} %param.16), kind=kOutput, calls=%fused_computation.13 | convolution fusion | flops 8503295 | bytes 164864 | tf_op jit(solution)/shard_map/dot_general | solution.py:98
  24.6 1.8 %fusion.7 = bf16[16,8,769]{2,1,0:T(8,128)(2,1)} fusion(bf16[16,8,769]{2,1,0:T(8,128)(2,1)} %fusion.5, bf16[256,128]{1,0:T(8,128)(2,1)} %param.18, bf16[128,256]{0,1:T(8,128)(2,1)S(1)} %all_gather.6, f32[256]{0:T(256)} %param.16), kind=kOutput, calls=%fused_computation.15 | convolution fusion | flops 8503296 | bytes 164864 | tf_op jit(solution)/shard_map/dot_general | solution.py:99
  26.3 1.8 %fusion.1 = bf16[16,8,769]{2,1,0:T(8,128)(2,1)} fusion(bf16[16,8,769]{2,1,0:T(8,128)(2,1)} %fusion.7, bf16[256,256]{1,0:T(8,128)(2,1)} %param.19, bf16[128,256]{0,1:T(8,128)(2,1)S(1)} %all_gather.6, f32[256]{0:T(256)} %param.16), kind=kOutput, calls=%fused_computation.7 | convolution fusion | flops 16908288 | bytes 263168 | tf_op jit(solution)/shard_map/dot_general | solution.py:100
  28.1 1.8 %fusion.3 = bf16[16,8,769]{2,1,0:T(8,128)(2,1)} fusion(bf16[16,8,769]{2,1,0:T(8,128)(2,1)} %fusion.1, bf16[256,256]{1,0:T(8,128)(2,1)} %param.20, bf16[128,256]{0,1:T(8,128)(2,1)S(1)} %all_gather.6, f32[256]{0:T(256)} %param.16), kind=kOutput, calls=%fused_computation.9 | convolution fusion | flops 16908288 | bytes 263168 | tf_op jit(solution)/shard_map/dot_general | solution.py:101
  30.0 0.6 constant_dynamic-update-slice_fusion
  30.6 6.8 %all-to-all-start = ((bf16[16,8,769]{2,1,0:T(8,128)(2,1)}), bf16[16,8,769]{2,1,0:T(8,128)(2,1)S(1)}, u32[]{:S(2)}, u32[]{:S(2)}) async-start(bf16[16,8,769]{2,1,0:T(8,128)(2,1)} %constant_dynamic-update-slice_fusion), calls=%async_computation | async-start | bytes 458752 | tf_op jit(solution)/shard_map/all_to_all | solution.py:19
  37.4 0.0 copy-start.8
  37.4 0.6 copy-done.8
  38.1 7.3 %all-to-all-done = bf16[16,8,769]{2,1,0:T(8,128)(2,1)S(1)} async-done(((bf16[16,8,769]{2,1,0:T(8,128)(2,1)}), bf16[16,8,769]{2,1,0:T(8,128)(2,1)S(1)}, u32[]{:S(2)}, u32[]{:S(2)}) %all-to-all-start) | async-done | bytes 196896 | tf_op jit(solution)/shard_map/all_to_all | solution.py:19
  45.4 0.1 fusion.44
  45.5 0.1 slice_multiply_fusion.2
  45.6 0.1 fusion.49
  45.7 0.1 maximum_bitcast_fusion
  45.8 0.1 fusion.47
  45.9 0.0 copy-done.2
  45.9 0.2 multiply_add_fusion
  46.1 0.0 copy-start.1
  46.1 0.5 fusion.8
  46.6 0.0 copy-start.5
  46.6 0.1 fusion.19
  46.7 0.1 fusion.21
  46.8 9.2 %all_to_all.30 = bf16[16,8,256]{2,1,0:T(8,128)(2,1)S(1)} all-to-all(bf16[16,8,256]{2,1,0:T(8,128)(2,1)S(1)} %broadcast_in_dim.4), channel_id=1, replica_groups=mesh['kv'=16,'tp'=16] {'kv'}, dimensions={0} | all-to-all | bytes 131072 | tf_op jit(solution)/shard_map/all_to_all | solution.py:36
  55.9 0.0 copy-done.5
  56.0 0.2 convolution_convert_fusion.3
  56.1 0.1 copy.37
  56.2 13.9 %all_to_all.31 = bf16[16,128,16]{1,2,0:T(8,128)(2,1)S(1)} all-to-all(bf16[16,128,16]{1,2,0:T(8,128)(2,1)S(1)} %bitcast.66), channel_id=1, replica_groups=mesh['kv'=16,'tp'=16] {'tp'}, dimensions={0} | all-to-all | bytes 131072 | tf_op jit(solution)/shard_map/all_to_all | solution.py:19
  70.2 0.0 copy-start.6
  70.2 0.7 copy-done.6
  70.9 14.9 %all_gather.7 = bf16[128,256]{0,1:T(8,128)(2,1)S(1)} all-gather(bf16[128,16]{0,1:T(8,128)(2,1)S(1)} %add_convert_fusion.1), channel_id=1, replica_groups=mesh['kv'=16,'tp'=16] {'tp'}, dimensions={1}, use_global_device_ids=true | all-gather | bytes 69632 | tf_op jit(solution)/shard_map/all_gather | solution.py:67
  85.7 0.1 fusion.14
  85.8 0.0 copy-start.7
  85.8 0.2 convert_element_type.142
  86.0 0.0 copy-done
  86.0 0.4 copy-done.7
  86.5 0.0 copy-start.3
  86.5 0.3 convolution_convert_fusion.1
  86.8 0.0 copy-done.1
  86.8 0.1 copy.38
  86.9 0.5 copy-done.3
  87.4 0.3 convolution_convert_fusion
  87.8 0.1 copy.39
  87.9 0.2 concatenate.65
  88.1 12.3 %all_to_all.32 = bf16[16,8,1409]{2,1,0:T(8,128)(2,1)S(1)} all-to-all(bf16[16,8,1409]{2,1,0:T(8,128)(2,1)S(1)} %concatenate.65), channel_id=1, replica_groups=mesh['kv'=16,'tp'=16] {'kv'}, dimensions={0} | all-to-all | bytes 721408 | tf_op jit(solution)/shard_map/all_to_all | solution.py:19
  100.4 0.1 convert_reduce_fusion
  100.5 0.1 fusion.41
  100.6 0.0 copy-start.4
  100.6 0.1 slice_multiply_fusion
  100.7 0.1 fusion.18
  100.8 10.4 %all_to_all.33 = bf16[16,8,704]{2,1,0:T(8,128)(2,1)S(1)} all-to-all(bf16[16,8,704]{2,1,0:T(8,128)(2,1)S(1)} %broadcast_in_dim.5), channel_id=1, replica_groups=mesh['kv'=16,'tp'=16] {'kv'}, dimensions={0} | all-to-all | bytes 360448 | tf_op jit(solution)/shard_map/all_to_all | solution.py:36
  111.1 0.0 copy-done.4
  111.1 0.2 convolution_convert_fusion.2
  111.4 0.1 copy.41
  111.5 14.3 %all_to_all.34 = bf16[16,128,16]{1,2,0:T(8,128)(2,1)S(1)} all-to-all(bf16[16,128,16]{1,2,0:T(8,128)(2,1)S(1)} %bitcast.67), channel_id=1, replica_groups=mesh['kv'=16,'tp'=16] {'tp'}, dimensions={0} | all-to-all | bytes 131072 | tf_op jit(solution)/shard_map/all_to_all | solution.py:19
  125.8 0.6 add_convert_fusion
  (11 shorter events, 0.1 us)
Async XLA Ops:
  0.6 85.4 %copy-start = (bf16[256,704]{0,1:T(8,128)(2,1)S(1)}, bf16[256,704]{0,1:T(8,128)(2,1)}, u32[]{:S(2)}) copy-start(bf16[256,704]{0,1:T(8,128)(2,1)} %param.23) | copy-start | bytes 1081348
  0.6 45.2 %copy-start.2 = (f32[8,1,128,256]{3,2,1,0:T(8,128)S(1)}, f32[8,1,128,256]{3,2,1,0:T(8,128)}, u32[]{:S(2)}) copy-start(f32[8,1,128,256]{3,2,1,0:T(8,128)} %param.15) | copy-start | bytes 3145732
  30.6 14.7 %all-to-all-start = ((bf16[16,8,769]{2,1,0:T(8,128)(2,1)}), bf16[16,8,769]{2,1,0:T(8,128)(2,1)S(1)}, u32[]{:S(2)}, u32[]{:S(2)}) async-start(bf16[16,8,769]{2,1,0:T(8,128)(2,1)} %constant_dynamic-update-slice_fusion), calls=%async_computation | async-start | bytes 458752 | tf_op jit(solution)/shard_map/all_to_all | solution.py:19
  37.4 0.7 copy-start.8
  46.1 40.7 %copy-start.1 = (f32[8,1,128,256]{3,2,1,0:T(8,128)}, f32[8,1,128,256]{3,2,1,0:T(8,128)S(1)}, u32[]{:S(2)}) copy-start(f32[8,1,128,256]{3,2,1,0:T(8,128)S(1)} %multiply_add_fusion) | copy-start | bytes 3145732
  46.6 9.4 %copy-start.5 = (bf16[256,256]{1,0:T(8,128)(2,1)S(1)}, bf16[256,256]{1,0:T(8,128)(2,1)}, u32[]{:S(2)}) copy-start(bf16[256,256]{1,0:T(8,128)(2,1)} %param.21) | copy-start | bytes 393220
  70.2 0.7 copy-start.6
  85.8 0.7 copy-start.7
  86.5 1.0 copy-start.3
  100.6 10.6 %copy-start.4 = (bf16[704,256]{1,0:T(8,128)(2,1)S(1)}, bf16[704,256]{1,0:T(8,128)(2,1)}, u32[]{:S(2)}) copy-start(bf16[704,256]{1,0:T(8,128)(2,1)} %param.25) | copy-start | bytes 1081348
where the time goes:
time: 127 us; the launch traced here: 126 us
  blocking collectives  96.8 us (76%)
  matrix products  8.66 us (7%)
  waiting for transfers between devices  7.25 us (6%)
  starting transfers between devices  6.75 us (5%)
  local copies, waits for them, and re-layouts  4.08 us (3%)
  other arithmetic  1.99 us (2%)
    all_to_all x3, blocking collectives, sent_and_summed(): lax.all_to_all(blocks, axis, split_axis=0, concat_axis=0, tiled=True)  40.5 us
    all_gather x2, blocking collectives, gathered_rows(): return lax.all_gather(columns, 'tp', axis=1, tiled=True)  36.7 us
    all_to_all x2, blocking collectives, copy_for_each(): lax.all_to_all(jnp.broadcast_to(value[None], (devices, *value.shape)), ax...  19.6 us
    all_to_all x1, waiting for transfers between devices, sent_and_summed(): lax.all_to_all(blocks, axis, split_axis=0, concat_axis=0, tiled=True)  7.25 us
    all_to_all x1, starting transfers between devices, sent_and_summed(): lax.all_to_all(blocks, axis, split_axis=0, concat_axis=0, tiled=True)  6.75 us
  transfers between devices with their start and end apart: 1, of which 1 were waited for; matrix products, arithmetic and copies ran while one was open for 0% of the time, Pallas kernels for 0%

commit v1 on v0

--- a/solution.py
+++ b/solution.py
@@ -6,6 +6,11 @@
 D = 4096
 HEADS = 16
 QK = 128
+
+
+def tiled_gather(x, axis, dim):
+    copies = jnp.concatenate([x] * lax.axis_size(axis), axis=dim)
+    return lax.all_to_all(copies, axis, dim, dim, tiled=True)
 
 
 def in_blocks(value, dim, devices):
@@ -64,7 +69,7 @@
 
 
 def gathered_rows(columns):
-    return lax.all_gather(columns, "tp", axis=1, tiled=True)
+    return tiled_gather(columns, "tp", 1)
 
 
 def owned_sums(partial_value, squares):

time: 127 us -> 114 us (0.90)
  blocking collectives: 96.8 us -> 85.4 us
  matrix products: 8.66 us -> 4.5 us
  local copies, waits for them, and re-layouts: 4.08 us -> 6.3 us
    all_gather x2 -> x0, blocking collectives: 36.7 us -> none  [gathered_rows(): return lax.all_gather(columns, 'tp', axis=1, tiled=True)]
    all_to_all x0 -> x2, blocking collectives: none -> 27.9 us  [tiled_gather(): return lax.all_to_all(copies, axis, dim, dim, tiled=True)]
    all_to_all x3, blocking collectives: 40.5 us -> 37.9 us  [sent_and_summed(): lax.all_to_all(blocks, axis, split_axis=0, concat_axis=0, tiled=True)]
    convert_element_type x0 -> x4, local copies, waits for them, and re-layouts: none -> 1.78 us  [the longest x2 0.89 us: on_device(): feature_block = gathered_rows(tokens).astype(jnp.float32)]
    unnamed x18 -> x57, local copies, waits for them, and re-layouts: 2.27 us -> 2.99 us
where the time goes in v1:
time: 114 us; the launch traced here: 113 us
  blocking collectives  85.4 us (75%)
  waiting for transfers between devices  7.3 us (6%)
  starting transfers between devices  6.76 us (6%)
  local copies, waits for them, and re-layouts  6.3 us (6%)
  matrix products  4.5 us (4%)
  other arithmetic  2 us (2%)
    all_to_all x3, blocking collectives, sent_and_summed(): lax.all_to_all(blocks, axis, split_axis=0, concat_axis=0, tiled=True)  37.9 us
    all_to_all x2, blocking collectives, tiled_gather(): return lax.all_to_all(copies, axis, dim, dim, tiled=True)  27.9 us
    all_to_all x2, blocking collectives, copy_for_each(): lax.all_to_all(jnp.broadcast_to(value[None], (devices, *value.shape)), ax...  19.6 us
    all_to_all x1, waiting for transfers between devices, sent_and_summed(): lax.all_to_all(blocks, axis, split_axis=0, concat_axis=0, tiled=True)  7.3 us
    all_to_all x1, starting transfers between devices, sent_and_summed(): lax.all_to_all(blocks, axis, split_axis=0, concat_axis=0, tiled=True)  6.76 us
    unnamed x57, local copies, waits for them, and re-layouts  2.99 us
  transfers between devices with their start and end apart: 1, of which 1 were waited for; matrix products, arithmetic and copies ran while one was open for 0% of the time, Pallas kernels for 0%

profile of v1, /device:TPU:1, one launch (start us, length us, event | category | flops | bytes accessed | tf_op | source)
XLA Modules:
  0.0 113.3 jit_solution(14538176227332757618)
XLA Ops:
  0.6 0.0 copy-start
  0.6 0.0 copy-start.2
  0.7 0.8 constant_dynamic-update-slice_fusion.15
  1.4 0.0 copy-done.2
  1.6 17.5 %all_to_all.48 = bf16[128,16,16]{0,2,1:T(8,128)(2,1)S(1)} all-to-all(bf16[128,16,16]{0,2,1:T(8,128)(2,1)S(1)} %bitcast.67), channel_id=1, replica_groups=mesh['kv'=16,'tp'=16] {'tp'}, dimensions={1} | all-to-all | bytes 131072 | tf_op jit(solution)/shard_map/all_to_all | solution.py:13
  19.1 0.1 multiply_reduce_fusion.1
  19.2 0.2 convert_element_type.171
  19.4 0.5 copy.39
  19.9 0.0 copy-start.12
  19.9 0.0 copy-start.9
  19.9 0.0 copy-start.10
  19.9 0.0 copy-start.6
  19.9 0.0 copy-start.7
  19.9 0.4 reshape.296
  20.4 0.2 copy-done.12
  20.6 0.2 copy-done.9
  20.7 0.8 fusion.3
  21.5 0.0 copy-done.10
  21.5 0.8 fusion.2
  22.3 0.0 copy-done.6
  22.3 0.8 fusion.1
  23.1 0.0 copy-done.7
  23.1 0.8 fusion
  23.9 0.6 constant_dynamic-update-slice_fusion.16
  24.5 6.8 %all-to-all-start.1 = ((bf16[16,8,769]{2,1,0:T(8,128)(2,1)}), bf16[16,8,769]{2,1,0:T(8,128)(2,1)S(1)}, u32[]{:S(2)}, u32[]{:S(2)}) async-start(bf16[16,8,769]{2,1,0:T(8,128)(2,1)} %constant_dynamic-update-slice_fusion.16), calls=%async_computation.1 | async-start | bytes 458752 | tf_op jit(solution)/shard_map/all_to_all | solution.py:24
  31.3 0.0 copy-start.13
  31.3 0.6 copy-done.13
  32.0 7.3 %all-to-all-done.1 = bf16[16,8,769]{2,1,0:T(8,128)(2,1)S(1)} async-done(((bf16[16,8,769]{2,1,0:T(8,128)(2,1)}), bf16[16,8,769]{2,1,0:T(8,128)(2,1)S(1)}, u32[]{:S(2)}, u32[]{:S(2)}) %all-to-all-start.1) | async-done | bytes 196896 | tf_op jit(solution)/shard_map/all_to_all | solution.py:24
  39.3 0.1 fusion.40
  39.4 0.1 slice_multiply_fusion.2
  39.5 0.1 fusion.45
  39.7 0.1 maximum_bitcast_fusion
  39.7 0.1 fusion.43
  39.8 0.2 multiply_add_fusion
  40.0 0.0 copy-start.1
  40.0 0.5 fusion.4
  40.5 0.1 fusion.15
  40.6 0.1 fusion.17
  40.7 9.2 %all_to_all.49 = bf16[16,8,256]{2,1,0:T(8,128)(2,1)S(1)} all-to-all(bf16[16,8,256]{2,1,0:T(8,128)(2,1)S(1)} %broadcast_in_dim.4), channel_id=1, replica_groups=mesh['kv'=16,'tp'=16] {'kv'}, dimensions={0} | all-to-all | bytes 131072 | tf_op jit(solution)/shard_map/all_to_all | solution.py:41
  49.9 0.2 convolution_convert_fusion.3
  50.1 0.1 copy.41
  50.2 12.9 %all_to_all.50 = bf16[16,128,16]{1,2,0:T(8,128)(2,1)S(1)} all-to-all(bf16[16,128,16]{1,2,0:T(8,128)(2,1)S(1)} %bitcast.64), channel_id=1, replica_groups=mesh['kv'=16,'tp'=16] {'tp'}, dimensions={0} | all-to-all | bytes 131072 | tf_op jit(solution)/shard_map/all_to_all | solution.py:24
  63.3 10.4 %all_to_all.51 = bf16[128,16,16]{0,2,1:T(8,128)(2,1)S(1)} all-to-all(bf16[128,16,16]{0,2,1:T(8,128)(2,1)S(1)} %bitcast.66), channel_id=1, replica_groups=mesh['kv'=16,'tp'=16] {'tp'}, dimensions={1} | all-to-all | bytes 131072 | tf_op jit(solution)/shard_map/all_to_all | solution.py:13
  73.7 0.1 multiply_reduce_fusion
  73.7 0.2 convert_element_type.172
  74.0 0.5 copy.42
  74.4 0.0 copy-start.11
  74.4 0.4 reshape.299
  74.9 0.2 copy-done.11
  75.1 0.3 convolution_convert_fusion
  75.4 0.7 copy-done.5
  76.1 0.3 convolution_convert_fusion.1
  76.4 0.2 concatenate.55
  76.6 12.3 %all_to_all.52 = bf16[16,8,1409]{2,1,0:T(8,128)(2,1)S(1)} all-to-all(bf16[16,8,1409]{2,1,0:T(8,128)(2,1)S(1)} %concatenate.55), channel_id=1, replica_groups=mesh['kv'=16,'tp'=16] {'kv'}, dimensions={0} | all-to-all | bytes 721408 | tf_op jit(solution)/shard_map/all_to_all | solution.py:24
  88.9 0.1 convert_reduce_fusion
  88.9 0.1 fusion.37
  89.1 0.1 slice_multiply_fusion
  89.1 0.1 fusion.14
  89.2 10.4 %all_to_all.53 = bf16[16,8,704]{2,1,0:T(8,128)(2,1)S(1)} all-to-all(bf16[16,8,704]{2,1,0:T(8,128)(2,1)S(1)} %broadcast_in_dim.5), channel_id=1, replica_groups=mesh['kv'=16,'tp'=16] {'kv'}, dimensions={0} | all-to-all | bytes 360448 | tf_op jit(solution)/shard_map/all_to_all | solution.py:41
  99.6 0.0 copy-done.4
  99.6 0.2 convolution_convert_fusion.2
  99.8 0.1 copy.44
  99.9 12.7 %all_to_all.54 = bf16[16,128,16]{1,2,0:T(8,128)(2,1)S(1)} all-to-all(bf16[16,128,16]{1,2,0:T(8,128)(2,1)S(1)} %bitcast.65), channel_id=1, replica_groups=mesh['kv'=16,'tp'=16] {'tp'}, dimensions={0} | all-to-all | bytes 131072 | tf_op jit(solution)/shard_map/all_to_all | solution.py:24
  112.7 0.6 add_convert_fusion
  (50 shorter events, 0.4 us)
Async XLA Ops:
  0.6 74.3 %copy-start = (bf16[256,704]{0,1:T(8,128)(2,1)S(1)}, bf16[256,704]{0,1:T(8,128)(2,1)}, u32[]{:S(2)}) copy-start(bf16[256,704]{0,1:T(8,128)(2,1)} %param.24) | copy-start | bytes 1081348
  0.6 0.8 copy-start.2
  19.9 0.7 copy-start.12
  19.9 0.8 copy-start.9
  19.9 1.6 %copy-start.10 = (bf16[256,128]{1,0:T(8,128)(2,1)S(1)}, bf16[256,128]{1,0:T(8,128)(2,1)}, u32[]{:S(2)}) copy-start(bf16[256,128]{1,0:T(8,128)(2,1)} %param.18) | copy-start | bytes 196612
  19.9 2.4 %copy-start.6 = (bf16[256,256]{1,0:T(8,128)(2,1)S(1)}, bf16[256,256]{1,0:T(8,128)(2,1)}, u32[]{:S(2)}) copy-start(bf16[256,256]{1,0:T(8,128)(2,1)} %param.19) | copy-start | bytes 393220
  19.9 3.2 %copy-start.7 = (bf16[256,256]{1,0:T(8,128)(2,1)S(1)}, bf16[256,256]{1,0:T(8,128)(2,1)}, u32[]{:S(2)}) copy-start(bf16[256,256]{1,0:T(8,128)(2,1)} %param.20) | copy-start | bytes 393220
  20.5 19.3 %copy-start.3 = (f32[8,1,128,256]{3,2,1,0:T(8,128)S(1)}, f32[8,1,128,256]{3,2,1,0:T(8,128)}, u32[]{:S(2)}) copy-start(f32[8,1,128,256]{3,2,1,0:T(8,128)} %param.15) | copy-start | bytes 3145732
  24.5 14.8 %all-to-all-start.1 = ((bf16[16,8,769]{2,1,0:T(8,128)(2,1)}), bf16[16,8,769]{2,1,0:T(8,128)(2,1)S(1)}, u32[]{:S(2)}, u32[]{:S(2)}) async-start(bf16[16,8,769]{2,1,0:T(8,128)(2,1)} %constant_dynamic-update-slice_fusion.16), calls=%async_computation.1 | async-start | bytes 458752 | tf_op jit(solution)/shard_map/all_to_all | solution.py:24
  31.3 0.7 copy-start.13
  40.0 33.7 %copy-start.1 = (f32[8,1,128,256]{3,2,1,0:T(8,128)}, f32[8,1,128,256]{3,2,1,0:T(8,128)S(1)}, u32[]{:S(2)}) copy-start(f32[8,1,128,256]{3,2,1,0:T(8,128)S(1)} %multiply_add_fusion) | copy-start | bytes 3145732
  40.5 9.4 %copy-start.8 = (bf16[256,256]{1,0:T(8,128)(2,1)S(1)}, bf16[256,256]{1,0:T(8,128)(2,1)}, u32[]{:S(2)}) copy-start(bf16[256,256]{1,0:T(8,128)(2,1)} %param.21) | copy-start | bytes 393220
  74.4 0.7 copy-start.11
  75.1 1.0 copy-start.5
  89.0 10.6 %copy-start.4 = (bf16[704,256]{1,0:T(8,128)(2,1)S(1)}, bf16[704,256]{1,0:T(8,128)(2,1)}, u32[]{:S(2)}) copy-start(bf16[704,256]{1,0:T(8,128)(2,1)} %param.25) | copy-start | bytes 1081348
